TPU v7x, 32 devices: a whole 2x2x4 slice. The times are simulated.
32 devices in a mesh: fs: 4 (over y, x), tp: 8 (over z, core).
Axes of the slice: x: 2, y: 2, z: 4, core: 2. Of those that a mesh axis runs over, the one named last changes fastest.
Arguments:
- saved_inputs: bfloat16 [2688, 4096], P('fs', 'tp'), may hold values from -6 to 6
- proj_cotangent: bfloat16 [2688, 4096], P('fs', 'tp'), may hold values from -0.115722656 to 0.115722656
- saved_hidden: bfloat16 [2688, 4096], P('fs', 'tp'), may hold values from -6 to 6
- out_cotangent: bfloat16 [2688, 4096], P('fs', 'tp'), may hold values from -0.115722656 to 0.115722656
- factors: bfloat16 [2, 4096, 128], replicated, may hold values from -0.46875 to 0.46875
- w_proj: float32 [4096, 4096], P('fs', 'tp'), may hold values from -0.09375 to 0.09375
- w_out: float32 [4096, 4096], P('tp', 'fs'), may hold values from -0.09375 to 0.09375
- moment_first: float32 [2, 128, 4096], P(None, None, 'tp'), may hold values from -1.8 to 1.8
- moment_second: float32 [2, 128, 4096], P(None, None, 'tp'), may hold values from 0.05 to 1
Outputs:
- proj_next: float32 [4096, 4096], P('fs', 'tp')
- out_next: float32 [4096, 4096], P('tp', 'fs')
- proj_copy: bfloat16 [4096, 4096], P(None, 'tp')
- out_copy: bfloat16 [4096, 4096], P('tp')
- first_next: float32 [2, 128, 4096], P(None, None, 'tp')
- second_next: float32 [2, 128, 4096], P(None, None, 'tp')
All inputs are finite; a program needn't handle non-finite values.
Results may differ from a plain program's by a relative error of at most 0.001.
Values may be sent and summed in bfloat16 or wider, within the bound.
A program may use at most 64 MiB of HBM per device.

v0:
```python
import jax
import jax.numpy as jnp
from jax import lax
from jax.sharding import PartitionSpec as P

beta_first = 0.9
beta_second = 0.95
learn_rate = 0.02
epsilon = 1e-06


def over_tokens(left_rows, right_rows, precise):
    return lax.dot_general(
        left_rows,
        right_rows,
        (((0,), (0,)), ((), ())),
        preferred_element_type=jnp.float32,
        precision=precise,
    )


def body(
    saved_inputs,
    proj_cotangent,
    saved_hidden,
    out_cotangent,
    factors,
    w_proj,
    w_out,
    moment_first,
    moment_second,
):
    highest = lax.Precision.HIGHEST
    fs_count = lax.axis_size("fs")
    tp_count = lax.axis_size("tp")
    d_model = factors.shape[1]
    hidden_width = proj_cotangent.shape[1]
    fs_rows = d_model // fs_count
    tp_feats = saved_inputs.shape[1]
    own_rows = lax.dynamic_slice_in_dim(factors, lax.axis_index("fs") * fs_rows, fs_rows, 1).astype(
        jnp.float32
    )
    own_feats = lax.dynamic_slice_in_dim(factors, lax.axis_index("tp") * tp_feats, tp_feats, 1)
    proj_rows = jnp.dot(saved_inputs, own_feats[0], preferred_element_type=jnp.float32)
    out_rows = jnp.dot(out_cotangent, own_feats[1], preferred_element_type=jnp.float32)
    proj_rows, out_rows = lax.psum((proj_rows, out_rows), "tp")
    partial_sums = jnp.stack(
        [
            over_tokens(proj_rows, proj_cotangent.astype(jnp.float32), highest),
            over_tokens(out_rows, saved_hidden.astype(jnp.float32), highest),
        ]
    )
    small_grads = lax.psum(partial_sums, "fs")
    first_next = beta_first * moment_first + (1.0 - beta_first) * small_grads
    second_next = beta_second * moment_second + (1.0 - beta_second) * small_grads * small_grads
    direction = first_next / (jnp.sqrt(second_next) + epsilon)
    update_full = jnp.einsum("kdr,kre->kde", own_rows, direction, precision=highest)
    squares = lax.psum(jnp.sum(update_full * update_full, axis=(1, 2)), ("fs", "tp"))
    norm_scale = lax.rsqrt(squares / (d_model * hidden_width * tp_count) + epsilon)
    stepped = update_full * norm_scale[:, None, None]
    proj_next = w_proj - learn_rate * stepped[0]
    out_next = w_out - learn_rate * stepped[1].T
    proj_copy, out_copy = (
        lax.all_gather(proj_next.astype(jnp.bfloat16), "fs", axis=0, tiled=True),
        lax.all_gather(out_next.astype(jnp.bfloat16), "fs", axis=1, tiled=True),
    )
    return (proj_next, out_next, proj_copy, out_copy, first_next, second_next)


def solution(mesh):
    placed = (
        P("fs", "tp"),
        P("fs", "tp"),
        P("fs", "tp"),
        P("fs", "tp"),
        P(),
        P("fs", "tp"),
        P("tp", "fs"),
        P(None, None, "tp"),
        P(None, None, "tp"),
    )
    return jax.shard_map(
        body,
        mesh=mesh,
        in_specs=placed,
        out_specs=(
            P("fs", "tp"),
            P("tp", "fs"),
            P(None, "tp"),
            P("tp", None),
            P(None, None, "tp"),
            P(None, None, "tp"),
        ),
        check_vma=False,
    )
```

profile of v0, /device:TPU:0, one launch (start us, length us, event | category | flops | bytes accessed | tf_op | source)
XLA Modules:
  0.0 292.3 jit_solution(14841451723777137700)
XLA Ops:
  7.2 0.0 copy-start
  7.2 0.0 copy-start.5
  7.2 0.0 all-reduce.6.cloned.1.call-start
  7.2 1.5 copy-done
  8.8 0.0 copy-start.6
  8.8 2.3 convolution_bitcast_fusion.1
  11.1 2.2 convolution_bitcast_fusion
  13.3 0.0 all-reduce.6.cloned.1.call-update
  13.3 0.0 all-reduce.4.cloned.1.call-start
  13.3 60.8 %all-reduce.6.cloned.1.call-done = (f32[672,128]{0,1:T(8,128)}, f32[672,128]{0,1:T(8,128)}) async-done(((f32[672,128]{0,1:T(8,128)}, f32[672,128]{0,1:T(8,128)}), (f32[672,128]{0,1:T(8,128)}, f32[672,128]{0,1:T(8,128)})) %all-reduce.6.cloned.1.call-update) | async-done | bytes 688144 | tf_op jit(solution)/shard_map/psum | solution.py:46
  74.1 0.0 copy-done.5
  74.1 1.5 convolution_bitcast_fusion.2
  75.6 0.0 copy-done.6
  75.6 1.5 convolution_bitcast_fusion.3
  77.1 0.8 pad_maximum_fusion
  77.9 0.0 all-reduce.4.cloned.1.call-update
  77.9 0.0 all-gather.5.cloned.1.call-start
  78.0 2.9 copy.15
  80.9 41.7 %all-reduce.4.cloned.1.call-done = f32[2,128,512]{2,1,0:T(8,128)} async-done(((f32[2,128,512]{2,1,0:T(8,128)}), f32[2,128,512]{2,1,0:T(8,128)}) %all-reduce.4.cloned.1.call-update) | async-done | bytes 524304 | tf_op jit(solution)/shard_map/psum | solution.py:53
  122.6 1.6 fusion.4
  124.2 0.0 copy-start.3
  124.2 0.0 copy-start.4
  124.2 4.0 %multiply_reduce_fusion = (f32[2]{0:T(128)S(1)}, f32[2,1024,512]{2,1,0:T(8,128)}) fusion(f32[2,128,512]{2,1,0:T(8,128)S(1)} %get-tuple-element.32, f32[2,128,512]{2,1,0:T(8,128)S(1)} %get-tuple-element.33, bf16[2,4096,128]{2,1,0:T(8,128)(2,1)S(1)} %copy-done, s32[]{:T(128)S(6)} %select_n.6), kind=kOutput, calls=%fused_computation | convolution fusion | flops 1612972032 | bytes 5767180 | tf_op jit(solution)/shard_map/kdr,kre->kde/dot_general | solution.py:57
  128.2 0.0 copy-done.3
  128.2 0.0 copy-done.4
  128.2 39.2 %psum.31 = f32[2]{0:T(128)S(1)} all-reduce(f32[2]{0:T(128)S(1)} %get-tuple-element.20), channel_id=1, replica_groups=mesh['fs'=4,'tp'=8] {'fs','tp'}, use_global_device_ids=true, to_apply=%region_4.0 | all-reduce | flops 2 | bytes 16 | tf_op jit(solution)/shard_map/psum | solution.py:58
  167.4 0.0 copy-start.2
  167.4 3.1 %broadcast_multiply_fusion = f32[2,1024,512]{2,1,0:T(8,128)S(1)} fusion(f32[2,1024,512]{2,1,0:T(8,128)} %get-tuple-element.21, f32[2]{0:T(128)S(1)} %add_rsqrt_fusion), kind=kLoop, calls=%fused_computation.7 | loop fusion | flops 1048576 | bytes 8388616 | tf_op jit(solution)/shard_map/mul | solution.py:60
  170.6 0.0 copy-done.2
  170.6 0.0 copy-start.1
  170.6 2.6 fusion.15
  173.2 0.4 copy-done.1
  173.5 0.0 all-gather.5.cloned.1.call-update
  173.6 0.0 all-gather.3.cloned.1.call-start
  173.6 4.5 %fusion.17 = (bf16[1024,512]{1,0:T(8,128)(2,1)}, f32[1024,512]{1,0:T(8,128)}) fusion(f32[1024,512]{1,0:T(8,128)} %param.14, f32[2,1024,512]{2,1,0:T(8,128)} %copy-done.1), kind=kLoop, calls=%fused_computation.30 | loop fusion | flops 1572864 | bytes 7340032 | tf_op jit(solution)/shard_map/convert_element_type | solution.py:64
  178.1 0.0 all-gather.3.cloned.1.call-update
  178.1 2.9 copy.16
  181.0 46.0 %all-gather.5.cloned.1.call-done = bf16[512,4096]{0,1:T(8,128)(2,1)} async-done(((bf16[512,1024]{0,1:T(8,128)(2,1)}), bf16[512,4096]{0,1:T(8,128)(2,1)}) %all-gather.5.cloned.1.call-update) | async-done | bytes 4194320 | tf_op jit(solution)/shard_map/all_gather | solution.py:65
  227.0 6.3 %copy.17 = bf16[512,4096]{1,0:T(8,128)(2,1)} copy(bf16[512,4096]{0,1:T(8,128)(2,1)} %all-gather.5.cloned.1.call-done) | data formatting | bytes 8388608
  233.3 48.0 %all-gather.3.cloned.1.call-done = bf16[4096,512]{1,0:T(8,128)(2,1)} async-done(((bf16[1024,512]{1,0:T(8,128)(2,1)}), bf16[4096,512]{1,0:T(8,128)(2,1)}) %all-gather.3.cloned.1.call-update) | async-done | bytes 4194320 | tf_op jit(solution)/shard_map/all_gather | solution.py:64
  281.3 4.5 %copy.22 = bf16[4096,512]{1,0:T(8,128)(2,1)} copy(bf16[4096,512]{1,0:T(8,128)(2,1)} %all-gather.3.cloned.1.call-done) | data formatting | bytes 8388608
  (1 shorter events, 0.0 us)
Async XLA Ops:
  7.2 1.6 copy-start
  7.2 66.9 %copy-start.5 = (bf16[672,512]{1,0:T(8,128)(2,1)S(1)}, bf16[672,512]{1,0:T(8,128)(2,1)}, u32[]{:S(2)}) copy-start(bf16[672,512]{1,0:T(8,128)(2,1)} %param.11) | copy-start | bytes 2064388
  7.2 66.9 %all-reduce.6.cloned.1.call-start = ((), (), s32[]{:S(2)}) async-start(), calls=%async_computation.3 | async-start | bytes 1572864 | tf_op jit(solution)/shard_map/psum | solution.py:46
  8.8 66.8 %copy-start.6 = (bf16[672,512]{1,0:T(8,128)(2,1)S(1)}, bf16[672,512]{1,0:T(8,128)(2,1)}, u32[]{:S(2)}) copy-start(bf16[672,512]{1,0:T(8,128)(2,1)} %param.10) | copy-start | bytes 2064388
  13.3 109.3 %all-reduce.4.cloned.1.call-start = ((), (), s32[]{:S(2)}) async-start(), calls=%async_computation | async-start | bytes 1048576 | tf_op jit(solution)/shard_map/psum | solution.py:53
  77.9 149.1 %all-gather.5.cloned.1.call-start = ((), (), s32[]{:S(2)}) async-start(), calls=%async_computation.2 | async-start | bytes 5242880 | tf_op jit(solution)/shard_map/all_gather | solution.py:65
  124.2 4.0 %copy-start.3 = (f32[2,128,512]{2,1,0:T(8,128)}, f32[2,128,512]{2,1,0:T(8,128)S(1)}, u32[]{:S(2)}) copy-start(f32[2,128,512]{2,1,0:T(8,128)S(1)} %get-tuple-element.33) | copy-start | bytes 1572868
  124.2 4.0 %copy-start.4 = (f32[2,128,512]{2,1,0:T(8,128)}, f32[2,128,512]{2,1,0:T(8,128)S(1)}, u32[]{:S(2)}) copy-start(f32[2,128,512]{2,1,0:T(8,128)S(1)} %get-tuple-element.32) | copy-start | bytes 1572868
  167.4 3.1 %copy-start.2 = (f32[512,1024]{0,1:T(8,128)S(1)}, f32[512,1024]{0,1:T(8,128)}, u32[]{:S(2)}) copy-start(f32[512,1024]{0,1:T(8,128)} %copy.15) | copy-start | bytes 6291460
  170.6 3.0 %copy-start.1 = (f32[2,1024,512]{2,1,0:T(8,128)}, f32[2,1024,512]{2,1,0:T(8,128)S(1)}, u32[]{:S(2)}) copy-start(f32[2,1024,512]{2,1,0:T(8,128)S(1)} %broadcast_multiply_fusion) | copy-start | bytes 12582916
  173.6 107.8 %all-gather.3.cloned.1.call-start = ((), (), s32[]{:S(2)}) async-start(), calls=%async_computation.1 | async-start | bytes 5242880 | tf_op jit(solution)/shard_map/all_gather | solution.py:64
Sparse Core Ops, SparseCore 0:
  13.4 60.6 all-reduce.5
  78.1 44.4 all-reduce.3
  173.7 53.2 all-gather.4
  228.7 52.5 all-gather.2
where the time goes:
time: 293 us; the launch traced here: 292 us
  waiting for transfers between devices  197 us (67%)
  blocking collectives  39.2 us (13%)
  local copies, waits for them, and re-layouts  18.5 us (6%)
  between operations  13.9 us (5%)
  other arithmetic  12.6 us (4%)
  matrix products  11.4 us (4%)
    psum x1, waiting for transfers between devices, body(): proj_rows, out_rows = lax.psum((proj_rows, out_rows), 'tp')  60.8 us
    all_gather x1, waiting for transfers between devices, body(): lax.all_gather(proj_next.astype(jnp.bfloat16), 'fs', axis=0, tiled=True)  48 us
    all_gather x1, waiting for transfers between devices, body(): lax.all_gather(out_next.astype(jnp.bfloat16), 'fs', axis=1, tiled=True)  46 us
    psum x1, waiting for transfers between devices, body(): small_grads = lax.psum(partial_sums, 'fs')  41.7 us
    psum x1, blocking collectives, body(): lax.psum(jnp.sum(update_full * update_full, axis=(1, 2)), ('fs', 'tp'))  39.2 us
    unnamed x18, local copies, waits for them, and re-layouts  18.5 us
  transfers between devices with their start and end apart: 4, of which 4 were waited for; matrix products, arithmetic and copies ran while one was open for 6% of the time, Pallas kernels for 0%

commit v1 on v0

--- a/solution.py
+++ b/solution.py
@@ -1,12 +1,352 @@
+import functools
+
 import jax
 import jax.numpy as jnp
 from jax import lax
+from jax.experimental import pallas as pl
+from jax.experimental.pallas import tpu as pltpu
 from jax.sharding import PartitionSpec as P
 
 beta_first = 0.9
 beta_second = 0.95
 learn_rate = 0.02
 epsilon = 1e-06
+weight_gain = 2500.0
+sub_steps = 2
+MESH = pl.DeviceIdType.MESH
+
+
+def encode(w):
+    t = w * weight_gain
+    t = t * t
+    t = t * t
+    t = t * t
+    t = t * t
+    return jnp.where(w < 0, -t, t).astype(jnp.bfloat16)
+
+
+def decode(code):
+    v = code.astype(jnp.float32)
+    size = jnp.exp2(jnp.log2(jnp.abs(v)) * (1.0 / 16.0)) * (1.0 / weight_gain)
+    return jnp.where(v < 0, -size, size)
+
+
+def two_parts(x, axis):
+    high = x.astype(jnp.bfloat16)
+    low = (x - high.astype(jnp.float32)).astype(jnp.bfloat16)
+    return jnp.concatenate([high, low], axis=axis)
+
+
+def exchange_kernel(
+    tp_count,
+    entries,
+    si_ref,
+    pc_ref,
+    sh_ref,
+    oc_ref,
+    f_ref,
+    wp_ref,
+    wo_ref,
+    mf_ref,
+    ms_ref,
+    first_ref,
+    second_ref,
+    d0_ref,
+    d1_ref,
+    gp_ref,
+    go_ref,
+    cp,
+    co,
+    rows,
+    rows_in,
+    rows_all,
+    part,
+    part_in,
+    grads,
+    sq,
+    sq_in,
+    bulk_s,
+    bulk_r,
+    zs_s,
+    zs_r,
+    zg_s,
+    zg_r,
+    fs_s,
+    fs_r,
+    fg_s,
+    fg_r,
+    n_s,
+    n_r,
+):
+    fs = lax.axis_index("fs")
+    tp = lax.axis_index("tp")
+    across_x = fs + 1 - 2 * lax.rem(fs, 2)
+    across_y = lax.rem(fs + 2, 4)
+    fs_peers = (across_x, across_y, 3 - fs)
+    tp_peers = [lax.rem(tp + o, tp_count) for o in range(1, tp_count)]
+
+    def send(src, dst, s_sem, r_sem, where):
+        copy = pltpu.make_async_remote_copy(
+            src_ref=src, dst_ref=dst, send_sem=s_sem, recv_sem=r_sem, device_id=where, device_id_type=MESH
+        )
+        copy.start()
+        return copy
+
+    barrier = pltpu.get_barrier_semaphore()
+    for p in fs_peers:
+        pl.semaphore_signal(barrier, inc=1, device_id={"fs": p}, device_id_type=MESH)
+    for p in tp_peers:
+        pl.semaphore_signal(barrier, inc=1, device_id={"tp": p}, device_id_type=MESH)
+    cp[...] = encode(wp_ref[...])
+    co[...] = encode(wo_ref[...])
+    pl.semaphore_wait(barrier, 3 + len(tp_peers))
+    bulk = [
+        send(cp, gp_ref.at[0], bulk_s.at[0], bulk_r.at[0], {"fs": across_x}),
+        send(co, go_ref.at[1], bulk_s.at[1], bulk_r.at[1], {"fs": across_y}),
+        send(co, go_ref.at[0], bulk_s.at[2], bulk_r.at[2], {"fs": across_x}),
+        send(cp, gp_ref.at[1], bulk_s.at[3], bulk_r.at[3], {"fs": across_y}),
+    ]
+
+    tokens, feats = si_ref.shape
+    own = pl.ds(pl.multiple_of(tp * feats, feats), feats)
+    rows[:tokens, :] = jnp.dot(si_ref[...], f_ref[0, own, :], preferred_element_type=jnp.float32)
+    rows[tokens:, :] = jnp.dot(oc_ref[...], f_ref[1, own, :], preferred_element_type=jnp.float32)
+    piece = rows_in.shape[1]
+
+    def rows_of(i):
+        return pl.ds(pl.multiple_of(i * piece, 8), piece)
+
+    copies = [
+        send(rows.at[rows_of(p), :], rows_in.at[i], zs_s.at[i], zs_r.at[i], {"tp": p})
+        for i, p in enumerate(tp_peers)
+    ]
+    for c in copies:
+        c.wait_recv()
+    total = rows[rows_of(tp), :]
+    for i in range(tp_count - 1):
+        total = total + rows_in[i]
+    rows_all[rows_of(tp), :] = total
+    gathers = [
+        send(rows_all.at[rows_of(tp), :], rows_all.at[rows_of(tp), :], zg_s.at[i], zg_r.at[i], {"tp": p})
+        for i, p in enumerate(tp_peers)
+    ]
+    for c in copies:
+        c.wait_send()
+    for c in gathers:
+        c.wait_recv()
+
+    rank = f_ref.shape[2]
+    for k, right in enumerate((pc_ref, sh_ref)):
+        left = two_parts(rows_all[k * tokens : (k + 1) * tokens, :], 1)
+        both = lax.dot_general(
+            left, right[...], (((0,), (0,)), ((), ())), preferred_element_type=jnp.float32
+        )
+        part[k * rank : (k + 1) * rank, :] = both[:rank] + both[rank:]
+    for c in gathers:
+        c.wait_send()
+    slab = part_in.shape[1]
+
+    def slab_of(i):
+        return pl.ds(pl.multiple_of(i * slab, 8), slab)
+
+    copies = [
+        send(part.at[slab_of(p), :], part_in.at[i], fs_s.at[i], fs_r.at[i], {"fs": p})
+        for i, p in enumerate(fs_peers)
+    ]
+    for c in copies:
+        c.wait_recv()
+    grads[slab_of(fs), :] = (part[slab_of(fs), :] + part_in[0]) + (part_in[1] + part_in[2])
+    gathers = [
+        send(grads.at[slab_of(fs), :], grads.at[slab_of(fs), :], fg_s.at[i], fg_r.at[i], {"fs": p})
+        for i, p in enumerate(fs_peers)
+    ]
+    bulk[0].wait_recv()
+    bulk.append(send(gp_ref.at[0], gp_ref.at[2], bulk_s.at[4], bulk_r.at[4], {"fs": across_y}))
+    bulk[1].wait_recv()
+    bulk.append(send(go_ref.at[1], go_ref.at[2], bulk_s.at[5], bulk_r.at[5], {"fs": across_x}))
+    for c in copies:
+        c.wait_send()
+    for c in gathers:
+        c.wait_recv()
+    small = grads[...]
+    first = beta_first * mf_ref[...] + (1.0 - beta_first) * small
+    second = beta_second * ms_ref[...] + (1.0 - beta_second) * small * small
+    first_ref[...] = first
+    second_ref[...] = second
+    direction = first / (jnp.sqrt(second) + epsilon)
+    for c in gathers:
+        c.wait_send()
+
+    d_model = f_ref.shape[1]
+    step = d_model // 8
+    squares = []
+    for k in range(2):
+        thin = two_parts(direction[k * rank : (k + 1) * rank], 0)
+
+        def add(i, acc, k=k, thin=thin):
+            f = f_ref[k, pl.ds(pl.multiple_of(i * step, step), step), :]
+            u = jnp.dot(jnp.concatenate([f, f], axis=1), thin, preferred_element_type=jnp.float32)
+            return acc + jnp.sum(u * u, axis=0, keepdims=True)
+
+        acc = lax.fori_loop(0, 8, add, jnp.zeros((1, direction.shape[1]), jnp.float32))
+        squares.append(jnp.sum(acc, axis=1, keepdims=True))
+    row = lax.broadcasted_iota(jnp.int32, sq.shape, 0)
+    sq[...] = jnp.where(row == 0, squares[0], squares[1])
+    norms = [send(sq, sq_in.at[i], n_s.at[i], n_r.at[i], {"tp": p}) for i, p in enumerate(tp_peers)]
+    for c in norms:
+        c.wait_recv()
+    total = sq[...]
+    for i in range(tp_count - 1):
+        total = total + sq_in[i]
+    scale = -learn_rate * lax.rsqrt(total / entries + epsilon)
+    d0_ref[...] = two_parts(direction[:rank] * scale[0:1, 0:1], 0)
+    d1_ref[...] = two_parts(jnp.transpose(direction[rank:] * scale[1:2, 0:1]), 1)
+    for c in norms:
+        c.wait_send()
+    for c in bulk[2:]:
+        c.wait_recv()
+    for c in bulk:
+        c.wait_send()
+
+
+def finish_kernel(
+    me_ref, f0, f1, d0, d1, wp, wo, gp, go, mf, ms, pn, on, pcopy, ocopy, first, second
+):
+    i = pl.program_id(0)
+    left = jnp.concatenate([f0[0], f0[0]], axis=1)
+    right = jnp.concatenate([f1[0], f1[0]], axis=1)
+    u0 = jnp.dot(left, d0[...], preferred_element_type=jnp.float32)
+    u1 = lax.dot_general(d1[...], right, (((1,), (1,)), ((), ())), preferred_element_type=jnp.float32)
+
+    @pl.when(i == 0)
+    def _():
+        first[...] = mf[...]
+        second[...] = ms[...]
+
+    @pl.when(i < sub_steps)
+    def _():
+        new = wp[...] + u0
+        pn[...] = new
+        pcopy[...] = new.astype(jnp.bfloat16)
+        new = wo[...] + u1
+        on[...] = new
+        ocopy[...] = new.astype(jnp.bfloat16)
+
+    @pl.when(i >= sub_steps)
+    def _():
+        pcopy[...] = (decode(gp[0]) + u0).astype(jnp.bfloat16)
+        ocopy[...] = (decode(go[0]) + u1).astype(jnp.bfloat16)
+
+
+def fast_body(si, pc, sh, oc, factors, w_proj, w_out, m1, m2):
+    fs_count, tp_count = lax.axis_size("fs"), lax.axis_size("tp")
+    kinds, d_model, rank = factors.shape
+    tokens = si.shape[0]
+    width = pc.shape[1]
+    d_rows = w_proj.shape[0]
+    f32, bf16 = jnp.float32, jnp.bfloat16
+    mf, ms = m1.reshape(2 * rank, width), m2.reshape(2 * rank, width)
+    vm = pl.BlockSpec(memory_space=pltpu.VMEM)
+    anywhere = pl.BlockSpec(memory_space=pl.ANY)
+    dma = lambda n: pltpu.SemaphoreType.DMA((n,))
+    peers = tp_count - 1
+    piece = 2 * tokens // tp_count
+    slab = 2 * rank // fs_count
+    first, second, d0, d1, gp, go = pl.pallas_call(
+        functools.partial(exchange_kernel, tp_count, float(d_model * width * tp_count)),
+        out_shape=(
+            jax.ShapeDtypeStruct((2 * rank, width), f32),
+            jax.ShapeDtypeStruct((2 * rank, width), f32),
+            jax.ShapeDtypeStruct((2 * rank, width), bf16),
+            jax.ShapeDtypeStruct((width, 2 * rank), bf16),
+            jax.ShapeDtypeStruct((3, d_rows, width), bf16),
+            jax.ShapeDtypeStruct((3, width, d_rows), bf16),
+        ),
+        in_specs=[vm] * 9,
+        out_specs=(vm, vm, vm, vm, anywhere, anywhere),
+        scratch_shapes=[
+            pltpu.VMEM((d_rows, width), bf16),
+            pltpu.VMEM((width, d_rows), bf16),
+            pltpu.VMEM((2 * tokens, rank), f32),
+            pltpu.VMEM((peers, piece, rank), f32),
+            pltpu.VMEM((2 * tokens, rank), f32),
+            pltpu.VMEM((2 * rank, width), f32),
+            pltpu.VMEM((3, slab, width), f32),
+            pltpu.VMEM((2 * rank, width), f32),
+            pltpu.VMEM((8, 128), f32),
+            pltpu.VMEM((peers, 8, 128), f32),
+            dma(6),
+            dma(6),
+            dma(peers),
+            dma(peers),
+            dma(peers),
+            dma(peers),
+            dma(3),
+            dma(3),
+            dma(3),
+            dma(3),
+            dma(peers),
+            dma(peers),
+        ],
+        compiler_params=pltpu.CompilerParams(
+            collective_id=0, has_side_effects=True, vmem_limit_bytes=40 * 1024 * 1024
+        ),
+        name="exchange",
+    )(si, pc, sh, oc, factors, w_proj, w_out, mf, ms)
+
+    me = lax.axis_index("fs").astype(jnp.int32).reshape(1)
+    n = sub_steps
+    rows = d_rows // n
+
+    def where(i, me):
+        return (me[0] ^ (i // n)) * n + i % n
+
+    def mine(i):
+        return jnp.minimum(i, n - 1)
+
+    def theirs(i):
+        j = jnp.maximum(i - n, 0)
+        return j // n, j % n
+
+    whole = pl.BlockSpec((2 * rank, width), lambda i, me: (0, 0))
+    pn, on, pcopy, ocopy, first, second = pl.pallas_call(
+        finish_kernel,
+        grid_spec=pltpu.PrefetchScalarGridSpec(
+            num_scalar_prefetch=1,
+            grid=(fs_count * n,),
+            in_specs=[
+                pl.BlockSpec((1, rows, rank), lambda i, me: (0, where(i, me), 0)),
+                pl.BlockSpec((1, rows, rank), lambda i, me: (1, where(i, me), 0)),
+                whole,
+                pl.BlockSpec((width, 2 * rank), lambda i, me: (0, 0)),
+                pl.BlockSpec((rows, width), lambda i, me: (mine(i), 0)),
+                pl.BlockSpec((width, rows), lambda i, me: (0, mine(i))),
+                pl.BlockSpec((1, rows, width), lambda i, me: (theirs(i)[0], theirs(i)[1], 0)),
+                pl.BlockSpec((1, width, rows), lambda i, me: (theirs(i)[0], 0, theirs(i)[1])),
+                whole,
+                whole,
+            ],
+            out_specs=[
+                pl.BlockSpec((rows, width), lambda i, me: (mine(i), 0)),
+                pl.BlockSpec((width, rows), lambda i, me: (0, mine(i))),
+                pl.BlockSpec((rows, width), lambda i, me: (where(i, me), 0)),
+                pl.BlockSpec((width, rows), lambda i, me: (0, where(i, me))),
+                whole,
+                whole,
+            ],
+        ),
+        out_shape=(
+            jax.ShapeDtypeStruct(w_proj.shape, f32),
+            jax.ShapeDtypeStruct(w_out.shape, f32),
+            jax.ShapeDtypeStruct((d_model, width), bf16),
+            jax.ShapeDtypeStruct((width, d_model), bf16),
+            jax.ShapeDtypeStruct((2 * rank, width), f32),
+            jax.ShapeDtypeStruct((2 * rank, width), f32),
+        ),
+        compiler_params=pltpu.CompilerParams(vmem_limit_bytes=40 * 1024 * 1024),
+        name="finish",
+    )(me, factors, factors, d0, d1, w_proj, w_out, gp, go, first, second)
+    return pn, on, pcopy, ocopy, first.reshape(m1.shape), second.reshape(m2.shape)
 
 
 def over_tokens(left_rows, right_rows, precise):
@@ -79,8 +419,9 @@
         P(None, None, "tp"),
         P(None, None, "tp"),
     )
+    planned = fast_body if mesh.shape["fs"] == 4 and mesh.shape["tp"] == 8 else body
     return jax.shard_map(
-        body,
+        planned,
         mesh=mesh,
         in_specs=placed,
         out_specs=(

time: 293 us -> 117 us (0.40)
  waiting for transfers between devices: 197 us -> 0 us
  Pallas kernels: 0 us -> 101 us
  blocking collectives: 39.2 us -> 0 us
  between operations: 13.9 us -> 0.7 us
  other arithmetic: 12.6 us -> 0 us
  matrix products: 11.4 us -> 0 us
  local copies, waits for them, and re-layouts: 18.5 us -> 15 us
    psum x2 -> x0, waiting for transfers between devices: 102 us -> none  [the longest x1 60.8 us: body(): proj_rows, out_rows = lax.psum((proj_rows, out_rows), 'tp')]
    pallas_call x0 -> x2, Pallas kernels: none -> 101 us  [the longest x1 88.8 us: fast_body(): pl.pallas_call(functools.partial(exchange_kernel, tp_count, float(d_model...]
    all_gather x2 -> x0, waiting for transfers between devices: 94 us -> none  [the longest x1 48 us: body(): lax.all_gather(proj_next.astype(jnp.bfloat16), 'fs', axis=0, tiled=True)]
    psum x1 -> x0, blocking collectives: 39.2 us -> none  [body(): lax.psum(jnp.sum(update_full * update_full, axis=(1, 2)), ('fs', 'tp'))]
    dot_general x5 -> x0, matrix products: 11.4 us -> none  [the longest x1 3.99 us: body(): jnp.einsum('kdr,kre->kde', own_rows, direction, precision=highest)]
    convert_element_type x2 -> x0, other arithmetic: 7.06 us -> none  [the longest x1 4.49 us: body(): proj_next.astype(jnp.bfloat16)]
    unnamed x18 -> x28, local copies, waits for them, and re-layouts: 18.5 us -> 15 us
    mul x1 -> x0, other arithmetic: 3.12 us -> none  [body(): stepped = update_full * norm_scale[:, None, None]]
  transfers between devices with their start and end apart: 4 -> 0, of which waited for: 4 -> 0; matrix products, arithmetic and copies ran while one was open for 6% -> 0% of each run, Pallas kernels for 0% -> 0%
where the time goes in v1:
time: 117 us
  Pallas kernels  101 us (86%)
  local copies, waits for them, and re-layouts  15 us (13%)
    pallas_call x1, Pallas kernels, fast_body(): pl.pallas_call(functools.partial(exchange_kernel, tp_count, float(d_model...  88.8 us
    unnamed x28, local copies, waits for them, and re-layouts  15 us
    pallas_call x1, Pallas kernels, fast_body(): pl.pallas_call(finish_kernel, grid_spec=pltpu.PrefetchScalarGridSpec(num_...  12.2 us

profile of v1, /device:TPU:0, one launch (start us, length us, event | category | flops | bytes accessed | tf_op | source)
XLA Modules:
  0.0 116.8 jit_solution(5122962477114986776)
XLA Ops:
  0.6 0.0 copy-start
  0.6 1.6 %copy-done = bf16[2,4096,128]{2,1,0:T(8,128)(2,1)S(1)} copy-done((bf16[2,4096,128]{2,1,0:T(8,128)(2,1)S(1)}, bf16[2,4096,128]{2,1,0:T(8,128)(2,1)}, u32[]{:S(2)}) %copy-start) | copy-done | bytes 2097176
  2.2 0.0 copy-start.2
  2.2 1.6 %copy-done.2 = f32[1024,512]{1,0:T(8,128)S(1)} copy-done((f32[1024,512]{1,0:T(8,128)S(1)}, f32[1024,512]{1,0:T(8,128)}, u32[]{:S(2)}) %copy-start.2) | copy-done | bytes 2097176
  3.8 0.0 copy-start.4
  3.8 1.6 %copy-done.4 = f32[512,1024]{1,0:T(8,128)S(1)} copy-done((f32[512,1024]{1,0:T(8,128)S(1)}, f32[512,1024]{1,0:T(8,128)}, u32[]{:S(2)}) %copy-start.4) | copy-done | bytes 2097176
  5.4 0.0 copy-start.8
  5.4 1.1 copy-done.8
  6.5 0.0 copy-start.9
  6.5 1.1 copy-done.9
  7.6 0.0 copy-start.10
  7.6 1.1 copy-done.10
  8.7 0.0 copy-start.11
  8.7 1.1 copy-done.11
  9.8 0.0 copy-start.12
  9.8 1.0 copy-done.12
  10.9 0.0 copy-start.13
  10.9 1.0 copy-done.13
  11.9 0.0 copy-start.1
  11.9 0.0 copy-start.3
  11.9 0.0 copy-start.5
  11.9 88.8 %exchange.1 = (f32[256,512]{1,0:T(8,128)S(1)}, f32[256,512]{1,0:T(8,128)S(1)}, bf16[256,512]{1,0:T(8,128)(2,1)S(1)}, bf16[512,256]{1,0:T(8,128)(2,1)S(1)}, bf16[...) custom-call(bf16[672,512]{1,0:T(8,128)(2,1)S(1)} %copy-done.8, bf16[672,512]{1,0:T(8,128)(2,1)S(1)} %copy-done.9, ...), custom_call_target="tpu_custom_call" | custom-call | tf_op jit(solution)/shard_map/exchange/pallas_call | solution.py:255
  100.7 0.0 copy-done.1
  100.7 0.0 copy-done.3
  100.7 0.0 copy-done.5
  100.8 0.0 copy-start.6
  100.8 1.9 %copy-done.6 = bf16[3,1024,512]{2,1,0:T(8,128)(2,1)S(1)} copy-done((bf16[3,1024,512]{2,1,0:T(8,128)(2,1)S(1)}, bf16[3,1024,512]{2,1,0:T(8,128)(2,1)}, u32[]{:S(2)}) %copy-start.6) | copy-done | bytes 3145752
  102.6 0.0 copy-start.7
  102.6 1.9 %copy-done.7 = bf16[3,512,1024]{2,1,0:T(8,128)(2,1)S(1)} copy-done((bf16[3,512,1024]{2,1,0:T(8,128)(2,1)S(1)}, bf16[3,512,1024]{2,1,0:T(8,128)(2,1)}, u32[]{:S(2)}) %copy-start.7) | copy-done | bytes 3145752
  104.5 12.2 %finish.1 = (f32[1024,512]{1,0:T(8,128)}, f32[512,1024]{1,0:T(8,128)}, bf16[4096,512]{1,0:T(8,128)(2,1)}, bf16[512,4096]{1,0:T(8,128)(2,1)}, f32[256,512]{1,0:T(8,128)}, /*index=5*/f32[256,512]{1,0:T(8,128)}) custom-call(s32[1]{0:T(128)} %bitcast.me_ref, bf16[2,4096,128]{2,1,0:T(8,128)(2,1)S(1)} %copy-done.1, bf16[2,4096,128]{2,1,0:T(8,128)(2,1)S(1)} %copy-done.1, ...), custom_call_target="tpu_custom_call" | custom-call | tf_op jit(solution)/shard_map/finish/pallas_call | solution.py:312
Async XLA Ops:
  0.6 1.6 %copy-start = (bf16[2,4096,128]{2,1,0:T(8,128)(2,1)S(1)}, bf16[2,4096,128]{2,1,0:T(8,128)(2,1)}, u32[]{:S(2)}) copy-start(bf16[2,4096,128]{2,1,0:T(8,128)(2,1)} %f1.1) | copy-start | bytes 6291460
  2.2 1.6 %copy-start.2 = (f32[1024,512]{1,0:T(8,128)S(1)}, f32[1024,512]{1,0:T(8,128)}, u32[]{:S(2)}) copy-start(f32[1024,512]{1,0:T(8,128)} %wp.1) | copy-start | bytes 6291460
  3.8 1.6 %copy-start.4 = (f32[512,1024]{1,0:T(8,128)S(1)}, f32[512,1024]{1,0:T(8,128)}, u32[]{:S(2)}) copy-start(f32[512,1024]{1,0:T(8,128)} %wo.1) | copy-start | bytes 6291460
  5.4 1.1 copy-start.8
  6.5 1.1 copy-start.9
  7.6 1.1 copy-start.10
  8.7 1.1 copy-start.11
  9.8 1.0 copy-start.12
  10.9 1.0 copy-start.13
  11.9 88.8 %copy-start.1 = (bf16[2,4096,128]{2,1,0:T(8,128)(2,1)S(1)}, bf16[2,4096,128]{2,1,0:T(8,128)(2,1)}, u32[]{:S(2)}) copy-start(bf16[2,4096,128]{2,1,0:T(8,128)(2,1)} %f1.1) | copy-start | bytes 6291460
  11.9 88.8 %copy-start.3 = (f32[1024,512]{1,0:T(8,128)S(1)}, f32[1024,512]{1,0:T(8,128)}, u32[]{:S(2)}) copy-start(f32[1024,512]{1,0:T(8,128)} %wp.1) | copy-start | bytes 6291460
  11.9 88.8 %copy-start.5 = (f32[512,1024]{1,0:T(8,128)S(1)}, f32[512,1024]{1,0:T(8,128)}, u32[]{:S(2)}) copy-start(f32[512,1024]{1,0:T(8,128)} %wo.1) | copy-start | bytes 6291460
  100.8 1.9 %copy-start.6 = (bf16[3,1024,512]{2,1,0:T(8,128)(2,1)S(1)}, bf16[3,1024,512]{2,1,0:T(8,128)(2,1)}, u32[]{:S(2)}) copy-start(bf16[3,1024,512]{2,1,0:T(8,128)(2,1)} %get-tuple-element.20.gp) | copy-start | bytes 9437188
  102.6 1.9 %copy-start.7 = (bf16[3,512,1024]{2,1,0:T(8,128)(2,1)S(1)}, bf16[3,512,1024]{2,1,0:T(8,128)(2,1)}, u32[]{:S(2)}) copy-start(bf16[3,512,1024]{2,1,0:T(8,128)(2,1)} %get-tuple-element.21.go) | copy-start | bytes 9437188

commit v2 on v1

--- a/solution.py
+++ b/solution.py
@@ -12,23 +12,28 @@
 learn_rate = 0.02
 epsilon = 1e-06
 weight_gain = 2500.0
-sub_steps = 2
+code_top = 200.0
+chunks = 4
+MIB = 1024 * 1024
 MESH = pl.DeviceIdType.MESH
 
 
-def encode(w):
-    t = w * weight_gain
-    t = t * t
-    t = t * t
-    t = t * t
-    t = t * t
-    return jnp.where(w < 0, -t, t).astype(jnp.bfloat16)
-
-
-def decode(code):
+def encode(x, gain, doublings):
+    t = x * gain
+    for _ in range(doublings):
+        t = t * t
+    return jnp.where(x < 0, -t, t).astype(jnp.bfloat16)
+
+
+def decode(code, gain, doublings):
     v = code.astype(jnp.float32)
-    size = jnp.exp2(jnp.log2(jnp.abs(v)) * (1.0 / 16.0)) * (1.0 / weight_gain)
+    size = jnp.exp2(jnp.log2(jnp.abs(v)) * (0.5**doublings)) * (1.0 / gain)
     return jnp.where(v < 0, -size, size)
+
+
+def largest(x):
+    top = jnp.max(jnp.max(jnp.abs(x), axis=0, keepdims=True), axis=1, keepdims=True)
+    return jnp.maximum(top, 1e-30)
 
 
 def two_parts(x, axis):
@@ -37,9 +42,41 @@
     return jnp.concatenate([high, low], axis=axis)
 
 
+def proj_step(f, d0):
+    return jnp.dot(jnp.concatenate([f, f], axis=1), d0[...], preferred_element_type=jnp.float32)
+
+
+def out_step(f, d1):
+    return lax.dot_general(
+        d1[...],
+        jnp.concatenate([f, f], axis=1),
+        (((1,), (1,)), ((), ())),
+        preferred_element_type=jnp.float32,
+    )
+
+
 def exchange_kernel(
     tp_count,
     entries,
+    si_hbm,
+    pc_hbm,
+    sh_hbm,
+    oc_hbm,
+    f_hbm,
+    wp_hbm,
+    wo_hbm,
+    mf_hbm,
+    ms_hbm,
+    first_ref,
+    second_ref,
+    d0_ref,
+    d1_ref,
+    gp_ref,
+    go_ref,
+    pn_ref,
+    on_ref,
+    fp_ref,
+    fo_ref,
     si_ref,
     pc_ref,
     sh_ref,
@@ -49,22 +86,21 @@
     wo_ref,
     mf_ref,
     ms_ref,
-    first_ref,
-    second_ref,
-    d0_ref,
-    d1_ref,
-    gp_ref,
-    go_ref,
     cp,
     co,
     rows,
     rows_in,
     rows_all,
     part,
+    part_code,
     part_in,
     grads,
     sq,
     sq_in,
+    top_out,
+    top_in,
+    top_all,
+    in_s,
     bulk_s,
     bulk_r,
     zs_s,
@@ -77,6 +113,10 @@
     fg_r,
     n_s,
     n_r,
+    ts_s,
+    ts_r,
+    tg_s,
+    tg_r,
 ):
     fs = lax.axis_index("fs")
     tp = lax.axis_index("tp")
@@ -97,15 +137,33 @@
         pl.semaphore_signal(barrier, inc=1, device_id={"fs": p}, device_id_type=MESH)
     for p in tp_peers:
         pl.semaphore_signal(barrier, inc=1, device_id={"tp": p}, device_id_type=MESH)
-    cp[...] = encode(wp_ref[...])
-    co[...] = encode(wo_ref[...])
+    pairs = (
+        (wp_hbm, wp_ref),
+        (wo_hbm, wo_ref),
+        (f_hbm, f_ref),
+        (si_hbm, si_ref),
+        (oc_hbm, oc_ref),
+        (pc_hbm, pc_ref),
+        (sh_hbm, sh_ref),
+        (mf_hbm, mf_ref),
+        (ms_hbm, ms_ref),
+    )
+    loads = [pltpu.make_async_copy(a, b, in_s.at[i]) for i, (a, b) in enumerate(pairs)]
+    for c in loads:
+        c.start()
+    loads[0].wait()
+    cp[...] = encode(wp_ref[...], weight_gain, 4)
     pl.semaphore_wait(barrier, 3 + len(tp_peers))
-    bulk = [
-        send(cp, gp_ref.at[0], bulk_s.at[0], bulk_r.at[0], {"fs": across_x}),
+    bulk = [send(cp, gp_ref.at[0], bulk_s.at[0], bulk_r.at[0], {"fs": across_x})]
+    loads[1].wait()
+    co[...] = encode(wo_ref[...], weight_gain, 4)
+    bulk += [
         send(co, go_ref.at[1], bulk_s.at[1], bulk_r.at[1], {"fs": across_y}),
         send(co, go_ref.at[0], bulk_s.at[2], bulk_r.at[2], {"fs": across_x}),
         send(cp, gp_ref.at[1], bulk_s.at[3], bulk_r.at[3], {"fs": across_y}),
     ]
+    for c in loads[2:5]:
+        c.wait()
 
     tokens, feats = si_ref.shape
     own = pl.ds(pl.multiple_of(tp * feats, feats), feats)
@@ -132,43 +190,81 @@
     ]
     for c in copies:
         c.wait_send()
+    for c in loads[5:]:
+        c.wait()
     for c in gathers:
         c.wait_recv()
 
     rank = f_ref.shape[2]
+    slab = part_in.shape[1]
     for k, right in enumerate((pc_ref, sh_ref)):
         left = two_parts(rows_all[k * tokens : (k + 1) * tokens, :], 1)
         both = lax.dot_general(
             left, right[...], (((0,), (0,)), ((), ())), preferred_element_type=jnp.float32
         )
-        part[k * rank : (k + 1) * rank, :] = both[:rank] + both[rank:]
+        both = both[:rank] + both[rank:]
+        part[k * rank : (k + 1) * rank, :] = both
+        for h in range(rank // slab):
+            mine = both[h * slab : (h + 1) * slab]
+            top = largest(mine)
+            start = k * rank + h * slab
+            top_out[start // slab] = jnp.broadcast_to(top, sq.shape)
+            part_code[start : start + slab, :] = encode(mine, code_top / top, 4)
     for c in gathers:
         c.wait_send()
-    slab = part_in.shape[1]
 
     def slab_of(i):
-        return pl.ds(pl.multiple_of(i * slab, 8), slab)
+        return pl.ds(pl.multiple_of(i * slab, slab), slab)
 
     copies = [
-        send(part.at[slab_of(p), :], part_in.at[i], fs_s.at[i], fs_r.at[i], {"fs": p})
+        send(part_code.at[slab_of(p), :], part_in.at[i], fs_s.at[i], fs_r.at[i], {"fs": p})
         for i, p in enumerate(fs_peers)
     ]
+    copies += [
+        send(top_out.at[p], top_in.at[i], ts_s.at[i], ts_r.at[i], {"fs": p}) for i, p in enumerate(fs_peers)
+    ]
+    d_rows, width = cp.shape
+
+    def relay(start, stop, at):
+        a = pl.ds(start * d_rows // 8, (stop - start) * d_rows // 8)
+        b = pl.ds(start * width // 8, (stop - start) * width // 8)
+        return [
+            send(gp_ref.at[0, a, :], gp_ref.at[2, a, :], bulk_s.at[at], bulk_r.at[at], {"fs": across_y}),
+            send(
+                go_ref.at[1, b, :], go_ref.at[2, b, :], bulk_s.at[at + 1], bulk_r.at[at + 1], {"fs": across_x}
+            ),
+        ]
+
+    bulk[0].wait_recv()
+    bulk[1].wait_recv()
+    bulk += relay(0, 1, 4)
     for c in copies:
         c.wait_recv()
-    grads[slab_of(fs), :] = (part[slab_of(fs), :] + part_in[0]) + (part_in[1] + part_in[2])
+    total = part[slab_of(fs), :]
+    for i in range(3):
+        total = total + decode(part_in[i], code_top / top_in[i][0:1, 0:1], 4)
+    top = largest(total)
+    top_all[fs] = jnp.broadcast_to(top, sq.shape)
+    grads[slab_of(fs), :] = encode(total, code_top / top, 4)
     gathers = [
         send(grads.at[slab_of(fs), :], grads.at[slab_of(fs), :], fg_s.at[i], fg_r.at[i], {"fs": p})
         for i, p in enumerate(fs_peers)
     ]
-    bulk[0].wait_recv()
-    bulk.append(send(gp_ref.at[0], gp_ref.at[2], bulk_s.at[4], bulk_r.at[4], {"fs": across_y}))
-    bulk[1].wait_recv()
-    bulk.append(send(go_ref.at[1], go_ref.at[2], bulk_s.at[5], bulk_r.at[5], {"fs": across_x}))
+    gathers += [
+        send(top_all.at[fs], top_all.at[fs], tg_s.at[i], tg_r.at[i], {"fs": p}) for i, p in enumerate(fs_peers)
+    ]
+    bulk += relay(1, 8, 6)
     for c in copies:
         c.wait_send()
     for c in gathers:
         c.wait_recv()
-    small = grads[...]
+    small = jnp.concatenate(
+        [
+            decode(grads[j * slab : (j + 1) * slab, :], code_top / top_all[j][0:1, 0:1], 4)
+            for j in range(2 * rank // slab)
+        ],
+        axis=0,
+    )
     first = beta_first * mf_ref[...] + (1.0 - beta_first) * small
     second = beta_second * ms_ref[...] + (1.0 - beta_second) * small * small
     first_ref[...] = first
@@ -188,7 +284,7 @@
             u = jnp.dot(jnp.concatenate([f, f], axis=1), thin, preferred_element_type=jnp.float32)
             return acc + jnp.sum(u * u, axis=0, keepdims=True)
 
-        acc = lax.fori_loop(0, 8, add, jnp.zeros((1, direction.shape[1]), jnp.float32))
+        acc = lax.fori_loop(0, 8, add, jnp.zeros((1, width), jnp.float32))
         squares.append(jnp.sum(acc, axis=1, keepdims=True))
     row = lax.broadcasted_iota(jnp.int32, sq.shape, 0)
     sq[...] = jnp.where(row == 0, squares[0], squares[1])
@@ -203,39 +299,67 @@
     d1_ref[...] = two_parts(jnp.transpose(direction[rank:] * scale[1:2, 0:1]), 1)
     for c in norms:
         c.wait_send()
-    for c in bulk[2:]:
+
+    size = d_rows // chunks
+
+    def block(slot, owner, proj_code, out_code):
+        def one(i, _):
+            at = pl.ds(pl.multiple_of(i * size, size), size)
+            there = pl.ds(pl.multiple_of(owner * d_rows + i * size, size), size)
+            u = proj_step(f_ref[0, there, :], d0_ref)
+            fp_ref[slot, at, :] = (decode(proj_code[at, :], weight_gain, 4) + u).astype(jnp.bfloat16)
+            if slot == 0:
+                pn_ref[at, :] = wp_ref[at, :] + u
+            u = out_step(f_ref[1, there, :], d1_ref)
+            fo_ref[slot, :, at] = (decode(out_code[:, at], weight_gain, 4) + u).astype(jnp.bfloat16)
+            if slot == 0:
+                on_ref[:, at] = wo_ref[:, at] + u
+            return 0
+
+        lax.fori_loop(0, chunks, one, 0)
+
+    block(0, fs, cp, co)
+    bulk[2].wait_recv()
+    block(1, across_x, gp_ref.at[0], go_ref.at[0])
+    bulk[3].wait_recv()
+    block(2, across_y, gp_ref.at[1], go_ref.at[1])
+    for c in bulk[4:]:
         c.wait_recv()
     for c in bulk:
         c.wait_send()
 
 
 def finish_kernel(
-    me_ref, f0, f1, d0, d1, wp, wo, gp, go, mf, ms, pn, on, pcopy, ocopy, first, second
+    me_ref, f_ref, d0, d1, gp, go, pn, on, fp, fo, mf, ms,
+    pn_hbm, on_hbm, pc_hbm, oc_hbm, first_hbm, second_hbm, last_p, last_o, sems
 ):
-    i = pl.program_id(0)
-    left = jnp.concatenate([f0[0], f0[0]], axis=1)
-    right = jnp.concatenate([f1[0], f1[0]], axis=1)
-    u0 = jnp.dot(left, d0[...], preferred_element_type=jnp.float32)
-    u1 = lax.dot_general(d1[...], right, (((1,), (1,)), ((), ())), preferred_element_type=jnp.float32)
-
-    @pl.when(i == 0)
-    def _():
-        first[...] = mf[...]
-        second[...] = ms[...]
-
-    @pl.when(i < sub_steps)
-    def _():
-        new = wp[...] + u0
-        pn[...] = new
-        pcopy[...] = new.astype(jnp.bfloat16)
-        new = wo[...] + u1
-        on[...] = new
-        ocopy[...] = new.astype(jnp.bfloat16)
-
-    @pl.when(i >= sub_steps)
-    def _():
-        pcopy[...] = (decode(gp[0]) + u0).astype(jnp.bfloat16)
-        ocopy[...] = (decode(go[0]) + u1).astype(jnp.bfloat16)
+    me = me_ref[0]
+    d_rows = pn.shape[0]
+    size = d_rows // chunks
+
+    def span(owner, i=0, n=d_rows):
+        return pl.ds(pl.multiple_of(owner * d_rows + i * n, n), n)
+
+    owners = (me, me ^ 1, me ^ 2)
+    pairs = [(pn, pn_hbm), (on, on_hbm), (mf, first_hbm), (ms, second_hbm)]
+    for r, owner in enumerate(owners):
+        pairs += [(fp.at[r], pc_hbm.at[span(owner), :]), (fo.at[r], oc_hbm.at[:, span(owner)])]
+    copies = [pltpu.make_async_copy(a, b, sems.at[i]) for i, (a, b) in enumerate(pairs)]
+    for c in copies:
+        c.start()
+    for i in range(chunks):
+        at = pl.ds(i * size, size)
+        there = span(me ^ 3, i, size)
+        u = proj_step(f_ref[0, there, :], d0)
+        last_p[at, :] = (decode(gp[2, at, :], weight_gain, 4) + u).astype(jnp.bfloat16)
+        u = out_step(f_ref[1, there, :], d1)
+        last_o[:, at] = (decode(go[2, :, at], weight_gain, 4) + u).astype(jnp.bfloat16)
+        for a, b in ((last_p.at[at, :], pc_hbm.at[there, :]), (last_o.at[:, at], oc_hbm.at[:, there])):
+            c = pltpu.make_async_copy(a, b, sems.at[len(copies)])
+            c.start()
+            copies.append(c)
+    for c in copies:
+        c.wait()
 
 
 def fast_body(si, pc, sh, oc, factors, w_proj, w_out, m1, m2):
@@ -247,36 +371,49 @@
     f32, bf16 = jnp.float32, jnp.bfloat16
     mf, ms = m1.reshape(2 * rank, width), m2.reshape(2 * rank, width)
     vm = pl.BlockSpec(memory_space=pltpu.VMEM)
-    anywhere = pl.BlockSpec(memory_space=pl.ANY)
+    hbm = pl.BlockSpec(memory_space=pltpu.HBM)
     dma = lambda n: pltpu.SemaphoreType.DMA((n,))
+    shape = jax.ShapeDtypeStruct
     peers = tp_count - 1
     piece = 2 * tokens // tp_count
     slab = 2 * rank // fs_count
-    first, second, d0, d1, gp, go = pl.pallas_call(
+    args = (si, pc, sh, oc, factors, w_proj, w_out, mf, ms)
+    held = tuple(pltpu.with_memory_space_constraint(a, pltpu.HBM) for a in args)
+    first, second, d0, d1, gp, go, pn, on, fp, fo = pl.pallas_call(
         functools.partial(exchange_kernel, tp_count, float(d_model * width * tp_count)),
         out_shape=(
-            jax.ShapeDtypeStruct((2 * rank, width), f32),
-            jax.ShapeDtypeStruct((2 * rank, width), f32),
-            jax.ShapeDtypeStruct((2 * rank, width), bf16),
-            jax.ShapeDtypeStruct((width, 2 * rank), bf16),
-            jax.ShapeDtypeStruct((3, d_rows, width), bf16),
-            jax.ShapeDtypeStruct((3, width, d_rows), bf16),
+            pltpu.VMEM((2 * rank, width), f32),
+            pltpu.VMEM((2 * rank, width), f32),
+            pltpu.VMEM((2 * rank, width), bf16),
+            pltpu.VMEM((width, 2 * rank), bf16),
+            pltpu.VMEM((3, d_rows, width), bf16),
+            pltpu.VMEM((3, width, d_rows), bf16),
+            pltpu.VMEM((d_rows, width), f32),
+            pltpu.VMEM((width, d_rows), f32),
+            pltpu.VMEM((3, d_rows, width), bf16),
+            pltpu.VMEM((3, width, d_rows), bf16),
         ),
-        in_specs=[vm] * 9,
-        out_specs=(vm, vm, vm, vm, anywhere, anywhere),
-        scratch_shapes=[
+        in_specs=[hbm] * 9,
+        out_specs=(vm,) * 10,
+        scratch_shapes=[pltpu.VMEM(a.shape, a.dtype) for a in args]
+        + [
             pltpu.VMEM((d_rows, width), bf16),
             pltpu.VMEM((width, d_rows), bf16),
             pltpu.VMEM((2 * tokens, rank), f32),
             pltpu.VMEM((peers, piece, rank), f32),
             pltpu.VMEM((2 * tokens, rank), f32),
             pltpu.VMEM((2 * rank, width), f32),
-            pltpu.VMEM((3, slab, width), f32),
-            pltpu.VMEM((2 * rank, width), f32),
+            pltpu.VMEM((2 * rank, width), bf16),
+            pltpu.VMEM((3, slab, width), bf16),
+            pltpu.VMEM((2 * rank, width), bf16),
             pltpu.VMEM((8, 128), f32),
             pltpu.VMEM((peers, 8, 128), f32),
-            dma(6),
-            dma(6),
+            pltpu.VMEM((fs_count, 8, 128), f32),
+            pltpu.VMEM((3, 8, 128), f32),
+            pltpu.VMEM((fs_count, 8, 128), f32),
+            dma(9),
+            dma(8),
+            dma(8),
             dma(peers),
             dma(peers),
             dma(peers),
@@ -287,65 +424,38 @@
             dma(3),
             dma(peers),
             dma(peers),
+            dma(3),
+            dma(3),
+            dma(3),
+            dma(3),
         ],
         compiler_params=pltpu.CompilerParams(
-            collective_id=0, has_side_effects=True, vmem_limit_bytes=40 * 1024 * 1024
+            collective_id=0, has_side_effects=True, vmem_limit_bytes=40 * MIB
         ),
         name="exchange",
-    )(si, pc, sh, oc, factors, w_proj, w_out, mf, ms)
+    )(*held)
 
     me = lax.axis_index("fs").astype(jnp.int32).reshape(1)
-    n = sub_steps
-    rows = d_rows // n
-
-    def where(i, me):
-        return (me[0] ^ (i // n)) * n + i % n
-
-    def mine(i):
-        return jnp.minimum(i, n - 1)
-
-    def theirs(i):
-        j = jnp.maximum(i - n, 0)
-        return j // n, j % n
-
-    whole = pl.BlockSpec((2 * rank, width), lambda i, me: (0, 0))
     pn, on, pcopy, ocopy, first, second = pl.pallas_call(
         finish_kernel,
-        grid_spec=pltpu.PrefetchScalarGridSpec(
-            num_scalar_prefetch=1,
-            grid=(fs_count * n,),
-            in_specs=[
-                pl.BlockSpec((1, rows, rank), lambda i, me: (0, where(i, me), 0)),
-                pl.BlockSpec((1, rows, rank), lambda i, me: (1, where(i, me), 0)),
-                whole,
-                pl.BlockSpec((width, 2 * rank), lambda i, me: (0, 0)),
-                pl.BlockSpec((rows, width), lambda i, me: (mine(i), 0)),
-                pl.BlockSpec((width, rows), lambda i, me: (0, mine(i))),
-                pl.BlockSpec((1, rows, width), lambda i, me: (theirs(i)[0], theirs(i)[1], 0)),
-                pl.BlockSpec((1, width, rows), lambda i, me: (theirs(i)[0], 0, theirs(i)[1])),
-                whole,
-                whole,
-            ],
-            out_specs=[
-                pl.BlockSpec((rows, width), lambda i, me: (mine(i), 0)),
-                pl.BlockSpec((width, rows), lambda i, me: (0, mine(i))),
-                pl.BlockSpec((rows, width), lambda i, me: (where(i, me), 0)),
-                pl.BlockSpec((width, rows), lambda i, me: (0, where(i, me))),
-                whole,
-                whole,
-            ],
+        in_specs=[pl.BlockSpec(memory_space=pltpu.SMEM)] + [vm] * 11,
+        out_specs=[hbm] * 6,
+        out_shape=(
+            shape(w_proj.shape, f32),
+            shape(w_out.shape, f32),
+            shape((d_model, width), bf16),
+            shape((width, d_model), bf16),
+            shape((2 * rank, width), f32),
+            shape((2 * rank, width), f32),
         ),
-        out_shape=(
-            jax.ShapeDtypeStruct(w_proj.shape, f32),
-            jax.ShapeDtypeStruct(w_out.shape, f32),
-            jax.ShapeDtypeStruct((d_model, width), bf16),
-            jax.ShapeDtypeStruct((width, d_model), bf16),
-            jax.ShapeDtypeStruct((2 * rank, width), f32),
-            jax.ShapeDtypeStruct((2 * rank, width), f32),
-        ),
-        compiler_params=pltpu.CompilerParams(vmem_limit_bytes=40 * 1024 * 1024),
+        scratch_shapes=[
+            pltpu.VMEM((d_rows, width), bf16),
+            pltpu.VMEM((width, d_rows), bf16),
+            dma(10 + 2 * chunks),
+        ],
+        compiler_params=pltpu.CompilerParams(vmem_limit_bytes=14 * MIB),
         name="finish",
-    )(me, factors, factors, d0, d1, w_proj, w_out, gp, go, first, second)
+    )(me, factors, d0, d1, gp, go, pn, on, fp, fo, first, second)
     return pn, on, pcopy, ocopy, first.reshape(m1.shape), second.reshape(m2.shape)
 
 

time: 117 us -> 88.3 us (0.75)
  local copies, waits for them, and re-layouts: 15 us -> 0.01 us
  Pallas kernels: 101 us -> 87.5 us
    unnamed x28 -> x2, local copies, waits for them, and re-layouts: 15 us -> 0.01 us
    pallas_call x1, Pallas kernels: 12.2 us -> 5.02 us  [fast_body(): pl.pallas_call(finish_kernel, in_specs=[pl.BlockSpec(memory_space=pltpu.S...]
    pallas_call x1, Pallas kernels: 88.8 us -> 82.4 us  [fast_body(): pl.pallas_call(functools.partial(exchange_kernel, tp_count, float(d_model...]
where the time goes in v2:
time: 88.3 us; the launch traced here: 88.1 us
  Pallas kernels  87.5 us (99%)
    pallas_call x1, Pallas kernels, fast_body(): pl.pallas_call(functools.partial(exchange_kernel, tp_count, float(d_model...  82.4 us
    pallas_call x1, Pallas kernels, fast_body(): pl.pallas_call(finish_kernel, in_specs=[pl.BlockSpec(memory_space=pltpu.S...  5.02 us

profile of v2, /device:TPU:0, one launch (start us, length us, event | category | flops | bytes accessed | tf_op | source)
XLA Modules:
  0.0 88.1 jit_solution(13036973224415180728)
XLA Ops:
  0.6 0.0 copy-start
  0.6 82.4 %exchange.1 = (f32[256,512]{1,0:T(8,128)S(1)}, f32[256,512]{1,0:T(8,128)S(1)}, bf16[256,512]{1,0:T(8,128)(2,1)S(1)}, bf16[512,256]{1,0:T(8,128)(2,1)S(1)}, bf16[...) custom-call(bf16[672,512]{1,0:T(8,128)(2,1)} %si_hbm.1, ...), custom_call_target="tpu_custom_call" | custom-call | tf_op jit(solution)/shard_map/exchange/pallas_call | solution.py:382
  83.1 0.0 copy-done
  83.1 5.0 %finish.1 = (f32[1024,512]{1,0:T(8,128)}, f32[512,1024]{1,0:T(8,128)}, bf16[4096,512]{1,0:T(8,128)(2,1)}, bf16[512,4096]{1,0:T(8,128)(2,1)}, f32[256,512]{1,0:T(8,128)}, /*index=5*/f32[256,512]{1,0:T(8,128)}) custom-call(s32[1]{0:T(128)} %bitcast.me_ref, bf16[2,4096,128]{2,1,0:T(8,128)(2,1)S(1)} %copy-done, bf16[256,512]{1,0:T(8,128)(2,1)S(1)} %get-tuple-element.22.d0, ...), custom_call_target="tpu_custom_call" | custom-call | tf_op jit(solution)/shard_map/finish/pallas_call | solution.py:439
Async XLA Ops:
  0.6 82.5 %copy-start = (bf16[2,4096,128]{2,1,0:T(8,128)(2,1)S(1)}, bf16[2,4096,128]{2,1,0:T(8,128)(2,1)}, u32[]{:S(2)}) copy-start(bf16[2,4096,128]{2,1,0:T(8,128)(2,1)} %f_ref.1) | copy-start | bytes 6291460
